TPU v7x, 32 devices: a whole 2x2x4 slice. The times are simulated.
32 devices in a mesh: ep: 8 (over z, x), tp: 4 (over y, core).
Axes of the slice: x: 2, y: 2, z: 4, core: 2. Of those that a mesh axis runs over, the one named last changes fastest.
Arguments:
- conv_value: bfloat16 [4096, 2048], P('ep', 'tp'), may hold values from -6 to 6
- conv_gate: bfloat16 [4096, 2048], P('ep', 'tp'), may hold values from -9 to 9
- conv_taps: float32 [31, 2048], P(None, 'tp'), may hold values from -14 to 14
- norm_gain: float32 [2048], P('tp'), may hold values from 0.1 to 1.9
- norm_shift: float32 [2048], P('tp'), may hold values from -3 to 3
- conv_out_weight: bfloat16 [2048, 2048], P(None, 'tp'), may hold values from -0.125 to 0.125
- moe_input: bfloat16 [1024, 2048], P('ep'), may hold values from -6 to 6
- moe_gain: float32 [2048], replicated, may hold values from 0.1 to 1.9
- routes: int32 [1024, 4], P('ep'), may hold values from 0 to 7, all different within a row; in each aligned block of 128 rows (0 to 127, 128 to 255, ...) at most 128 rows name the same one
- route_weights: float32 [1024, 4], P('ep'), may hold values from 0.25 to 1
- expert_gate: bfloat16 [8, 2048, 4096], P('ep', None, 'tp'), may hold values from -0.125 to 0.125
- expert_up: bfloat16 [8, 2048, 4096], P('ep', None, 'tp'), may hold values from -0.125 to 0.125
- expert_down: bfloat16 [8, 4096, 2048], P('ep', None, 'tp'), may hold values from -0.09375 to 0.09375
- shared_gate: bfloat16 [2048, 512], P(None, 'tp'), may hold values from -0.125 to 0.125
- shared_up: bfloat16 [2048, 512], P(None, 'tp'), may hold values from -0.125 to 0.125
- shared_down: bfloat16 [512, 2048], P(None, 'tp'), may hold values from -0.25 to 0.25
Outputs:
- conv_result: bfloat16 [4096, 2048], P('ep', 'tp')
- moe_result: bfloat16 [1024, 2048], P('ep', 'tp')
Inputs may be any that keep to these rules, and one draw needn't show every extreme that they name: `routes`: in the rows of one device (aligned blocks of 128 rows) no expert is named by more than 128 rows, a bound that some block reaches; each row names 4 different experts.
All inputs are finite; a program needn't handle non-finite values.
Results may differ from a plain program's by a relative error of at most 0.0068.
Values may be sent and summed in bfloat16 or wider, within the bound.
A program may use at most 64 MiB of HBM per device.

v0:
```python
import functools

import jax
import jax.numpy as jnp
from jax import lax
from jax.experimental import pallas as pl
from jax.experimental.pallas import tpu as pltpu
from jax.sharding import PartitionSpec as P

MESH = pl.DeviceIdType.MESH
TILES = 2
CHUNK = 64


def from_behind(value, axis, steps):
    count = lax.axis_size(axis)
    initial, last = (max(0, -steps), min(count, count - steps))
    return lax.ppermute(value, axis, [(source, source + steps) for source in range(initial, last)])


def silu(v):
    return v / (1.0 + jnp.exp(-v))


def moe_kernel(
    depth,
    normed,
    weights,
    gate_hbm,
    up_hbm,
    down_hbm,
    sgate_hbm,
    sup_hbm,
    sdown_hbm,
    value_hbm,
    cgate_hbm,
    cweight_hbm,
    taps,
    gain,
    shift,
    conv_out,
    out,
    sgate,
    sup,
    sdown,
    value,
    cgate,
    cweight,
    padded,
    filtered,
    stats,
    tail,
    halo,
    rowsums,
    chidden,
    gate,
    up,
    down,
    tokens,
    hidden,
    returned,
    outgoing,
    shidden,
    load_sem,
    own_sem,
    ssend,
    srecv,
    tsend,
    trecv,
    fsend,
    frecv,
    ysend,
    yrecv,
    psend,
    precv,
    gsend,
    grecv,
    rsend,
    rrecv,
    msend,
    mrecv,
    csend,
    crecv,
):
    e = lax.axis_index("ep")
    q = lax.axis_index("tp")
    z, x = e // 2, e % 2
    y, c = q // 2, q % 2
    sister = (e, y * 2 + (1 - c))
    across = (e, (1 - y) * 2 + c)
    beside = (z * 2 + (1 - x), q)
    rows, width = normed.shape
    half = width // 2
    far = (1 - y) * 2 + c

    def home(s, a):
        return (((z + s) % depth) * 2 + (x if a == 0 else 1 - x), q)

    def copy(src, dst, send, recv, device):
        return pltpu.make_async_remote_copy(
            src_ref=src, dst_ref=dst, send_sem=send, recv_sem=recv, device_id=device, device_id_type=MESH
        )

    loads = [
        pltpu.make_async_copy(src, dst, load_sem.at[i])
        for i, (src, dst) in enumerate(
            (
                (value_hbm, value),
                (cgate_hbm, cgate),
                (sgate_hbm, sgate),
                (sup_hbm, sup),
                (gate_hbm.at[0], gate),
                (up_hbm.at[0], up),
                (cweight_hbm, cweight),
                (down_hbm.at[0], down),
                (sdown_hbm, sdown),
            )
        )
    ]
    for load in loads:
        load.start()
    own = [
        pltpu.make_async_copy(normed.at[:, h * half : (h + 1) * half], tokens.at[0, h, 0], own_sem.at[h])
        for h in range(2)
    ]
    for load in own:
        load.start()

    peers = [home(s, a) for s in range(depth) for a in range(2) if (s, a) != (0, 0)]
    peers += [(e, (q + k) % 4) for k in range(1, 4)]
    barrier = pltpu.get_barrier_semaphore()
    for peer in peers:
        pl.semaphore_signal(barrier, inc=1, device_id=peer, device_id_type=MESH)
    pl.semaphore_wait(barrier, len(peers))

    pending = []

    def launch(cp):
        cp.start()
        pending.append(cp)
        return cp

    for load in own:
        load.wait()
    mine = tokens.at[0, c, 0]
    arrive = {}
    arrive[0, 1] = launch(copy(mine, tokens.at[0, c, 1], tsend.at[0, 1], trecv.at[0, 1], beside))
    for s in range(1, depth):
        target = (((z + depth - s) % depth) * 2 + x, q)
        arrive[s, 0] = launch(copy(mine, tokens.at[s, c, 0], tsend.at[s, 0], trecv.at[s, 0], target))

    rows_a, channels = value.shape
    tap_count, edge = taps.shape[0], halo.shape[0]
    lead = edge - (tap_count - 1)
    chunks = rows_a // CHUNK

    def chunk_of(i):
        return pl.multiple_of(i * CHUNK, CHUNK)

    def glu(i, carry):
        at = pl.ds(chunk_of(i), CHUNK)
        gated = value[at, :].astype(jnp.float32) * (1.0 / (1.0 + jnp.exp(-cgate[at, :].astype(jnp.float32))))
        rounded = gated.astype(jnp.bfloat16).astype(jnp.float32)
        padded[pl.ds(pl.multiple_of(i * CHUNK + edge, 8), CHUNK), :] = rounded
        return carry

    loads[0].wait()
    loads[1].wait()
    lax.fori_loop(0, chunks, glu, 0)
    tail[...] = padded[rows_a:, :].astype(jnp.bfloat16)
    count = 2 * depth
    edge_copy = launch(copy(tail, halo, csend.at[0], crecv.at[0], ((e + 1) % count, q)))

    loads[2].wait()
    loads[3].wait()
    shared_gate = jnp.dot(normed[...], sgate[...], preferred_element_type=jnp.float32)
    shared_up = jnp.dot(normed[...], sup[...], preferred_element_type=jnp.float32)
    shidden[q] = (silu(shared_gate) * shared_up).astype(jnp.bfloat16)

    swapped = {}

    def pass_on(s, a):
        arrive[s, a].wait_recv()
        block = tokens.at[s, c, a]
        if a == 0:
            arrive[s, 1] = launch(copy(block, tokens.at[s, c, 1], tsend.at[s, 1], trecv.at[s, 1], beside))
        swapped[s, a] = launch(copy(block, tokens.at[s, c, a], fsend.at[s, a], frecv.at[s, a], sister))

    tile = hidden.shape[4]
    ycopies, pcopies = {}, {}

    def first(s):
        for t in range(TILES):
            cols = slice(t * tile, (t + 1) * tile)

            def product(weight):
                total = None
                for h in range(2):
                    block = tokens[s, h].reshape(2 * rows, half)
                    part = jnp.dot(block, weight[h * half : (h + 1) * half, cols], preferred_element_type=jnp.float32)
                    total = part if total is None else total + part
                return total

            hidden[s, q, t] = (silu(product(gate)) * product(up)).astype(jnp.bfloat16)
            block = hidden.at[s, q, t]
            ycopies[s, t] = launch(copy(block, hidden.at[s, q, t], ysend.at[s, t], yrecv.at[s, t], across))
            pcopies[s, t] = launch(copy(block, hidden.at[s, q, t], psend.at[s, t], precv.at[s, t], sister))

    pass_on(0, 1)
    pass_on(1, 0)
    swapped[0, 1].wait_recv()
    loads[4].wait()
    loads[5].wait()
    first(0)

    edge_copy.wait_recv()
    padded[0:edge, :] = jnp.where(e == 0, 0.0, halo[...].astype(jnp.float32))
    lane = lax.broadcasted_iota(jnp.int32, (CHUNK, 128), 1)

    def convolve(i, carry):
        start = chunk_of(i)
        at = pl.ds(start, CHUNK)
        sums, squares = jnp.zeros((CHUNK, 128), jnp.float32), jnp.zeros((CHUNK, 128), jnp.float32)
        for column in range(0, channels, 128):
            cols = slice(column, column + 128)
            window = padded[pl.ds(start, CHUNK + edge), cols]
            total = jnp.zeros((CHUNK, 128), jnp.float32)
            for b in range(8):
                size = CHUNK + (8 if b else 0)
                part = None
                for a in range(edge // 8 + 1):
                    j = 8 * a + b - lead
                    if 0 <= j < tap_count:
                        term = taps[j : j + 1, cols] * window[8 * a : 8 * a + size]
                        part = term if part is None else part + term
                if b:
                    part = pltpu.roll(part, size - b, 0)[:CHUNK]
                total = total + part
            filtered[at, cols] = total
            sums = sums + total
            squares = squares + total * total
        row_sum = jnp.sum(sums, axis=1, keepdims=True)
        row_squares = jnp.sum(squares, axis=1, keepdims=True)
        stats[at, :] = jnp.where(lane == 0, row_sum, jnp.where(lane == 1, row_squares, 0.0))
        return carry

    lax.fori_loop(0, chunks, convolve, 0)
    rowsums[q] = stats[...].T[:8]
    mcopies = [
        launch(copy(rowsums.at[q], rowsums.at[q], msend.at[k - 1], mrecv.at[k - 1], (e, (q + k) % 4)))
        for k in range(1, 4)
    ]

    scopies = []
    for k in range(1, 4):
        scopies.append(
            launch(copy(shidden.at[q], shidden.at[q], ssend.at[k - 1], srecv.at[k - 1], (e, (q + k) % 4)))
        )
    for s in range(1, depth):
        if s + 1 < depth:
            pass_on(s + 1, 0)
        pass_on(s, 1)
        swapped[s, 0].wait_recv()
        swapped[s, 1].wait_recv()
        first(s)
        if s == 1:
            for cp in mcopies:
                cp.wait_recv()
            whole = rowsums[0] + rowsums[1] + rowsums[2] + rowsums[3]
            stats[...] = jnp.concatenate([whole, jnp.zeros((120, rows_a), jnp.float32)], axis=0).T
            total_channels = channels * 4

            def normalise(i, carry):
                at = pl.ds(chunk_of(i), CHUNK)
                both = stats[at, :] / total_channels
                mean, square = both[:, 0:1], both[:, 1:2]
                scaled = (filtered[at, :] - mean) * lax.rsqrt(square - mean * mean + 1e-05)
                chidden[q, at, :] = silu(scaled * gain[...] + shift[...]).astype(jnp.bfloat16)
                return carry

            lax.fori_loop(0, chunks, normalise, 0)
            cacross = launch(copy(chidden.at[q], chidden.at[q], csend.at[1], crecv.at[1], across))
            csister = launch(copy(chidden.at[q], chidden.at[q], csend.at[2], crecv.at[2], sister))

    cacross.wait_recv()
    cpassed = launch(copy(chidden.at[far], chidden.at[far], csend.at[3], crecv.at[3], sister))
    csister.wait_recv()
    loads[6].wait()
    cpassed.wait_recv()

    def project(i, carry):
        at = pl.ds(pl.multiple_of(i * 256, 256), 256)
        product = None
        for k in range(4):
            part = jnp.dot(
                chidden[k, at, :],
                cweight[k * channels : (k + 1) * channels, :],
                preferred_element_type=jnp.float32,
            )
            product = part if product is None else product + part
        conv_out[at, :] = product.astype(jnp.bfloat16)
        return carry

    lax.fori_loop(0, rows_a // 256, project, 0)
    loads[7].wait()
    homes = {}
    for s in range(depth):
        forwards = []
        for t in range(TILES):
            ycopies[s, t].wait_recv()
            forwards.append(
                launch(copy(hidden.at[s, far, t], hidden.at[s, far, t], gsend.at[s, t], grecv.at[s, t], sister))
            )
            pcopies[s, t].wait_recv()
        for forward in forwards:
            forward.wait_recv()
        total = None
        for k in range(4):
            for t in range(TILES):
                at = (k * TILES + t) * tile
                part = jnp.dot(hidden[s, k, t], down[at : at + tile, :], preferred_element_type=jnp.float32)
                total = part if total is None else total + part
        for a in range(2):
            piece = total[a * rows : (a + 1) * rows].astype(jnp.bfloat16)
            if (s, a) == (0, 0):
                returned[0, 0] = piece
            else:
                outgoing[s, a] = piece
                homes[s, a] = launch(
                    copy(outgoing.at[s, a], returned.at[s, a], rsend.at[s, a], rrecv.at[s, a], home(s, a))
                )

    for cp in scopies:
        cp.wait_recv()
    loads[8].wait()
    moe_sum = None
    share = shidden.shape[2]
    for k in range(4):
        part = jnp.dot(shidden[k], sdown[k * share : (k + 1) * share, :], preferred_element_type=jnp.float32)
        moe_sum = part if moe_sum is None else moe_sum + part
    for s in range(depth):
        for a in range(2):
            if (s, a) != (0, 0):
                homes[s, a].wait_recv()
            at = s * 2 + a
            moe_sum = moe_sum + weights[:, at : at + 1] * returned[s, a].astype(jnp.float32)
    out[...] = moe_sum.astype(jnp.bfloat16)
    for cp in pending:
        cp.wait_send()


def fused(
    conv, normed, routes, route_weights, expert_gate, expert_up, expert_down, shared_gate, shared_up, shared_down
):
    value, cgate, taps, gain, shift, cweight = conv
    rows_a, channels = value.shape
    edge = -(-(taps.shape[0] - 1) // 8) * 8
    rows, width = normed.shape
    depth = lax.axis_size("ep") // 2
    e = lax.axis_index("ep")
    z, x = e // 2, e % 2
    source = jnp.stack([((z + depth - s) % depth) * 2 + (x + a) % 2 for s in range(depth) for a in range(2)])
    weights = jnp.sum(
        jnp.where(routes[:, :, None] == source[None, None, :], route_weights[:, :, None], 0.0), axis=1
    )
    units, columns = expert_gate.shape[2], expert_down.shape[2]
    tile = units // TILES
    bf = jnp.bfloat16
    vmem = pl.BlockSpec(memory_space=pltpu.VMEM)
    hbm = pl.BlockSpec(memory_space=pl.ANY)
    dma = pltpu.SemaphoreType.DMA
    pairs = (depth, 2)
    flops = 2 * depth * 2 * rows * (2 * width * units + 4 * units * columns)
    return pl.pallas_call(
        functools.partial(moe_kernel, depth),
        out_shape=(
            jax.ShapeDtypeStruct((rows_a, cweight.shape[1]), bf),
            jax.ShapeDtypeStruct((rows, columns), bf),
        ),
        in_specs=[vmem] * 2 + [hbm] * 9 + [vmem] * 3,
        out_specs=(vmem, vmem),
        scratch_shapes=[
            pltpu.VMEM(shared_gate.shape, bf),
            pltpu.VMEM(shared_up.shape, bf),
            pltpu.VMEM(shared_down.shape, bf),
            pltpu.VMEM(value.shape, bf),
            pltpu.VMEM(cgate.shape, bf),
            pltpu.VMEM(cweight.shape, bf),
            pltpu.VMEM((rows_a + edge, channels), jnp.float32),
            pltpu.VMEM((rows_a, channels), jnp.float32),
            pltpu.VMEM((rows_a, 128), jnp.float32),
            pltpu.VMEM((edge, channels), bf),
            pltpu.VMEM((edge, channels), bf),
            pltpu.VMEM((4, 8, rows_a), jnp.float32),
            pltpu.VMEM((4, rows_a, channels), bf),
            pltpu.VMEM(expert_gate.shape[1:], bf),
            pltpu.VMEM(expert_up.shape[1:], bf),
            pltpu.VMEM(expert_down.shape[1:], bf),
            pltpu.VMEM((depth, 2, 2, rows, width // 2), bf),
            pltpu.VMEM((depth, 4, TILES, 2 * rows, tile), bf),
            pltpu.VMEM((depth, 2, rows, columns), bf),
            pltpu.VMEM((depth, 2, rows, columns), bf),
            pltpu.VMEM((4, rows, shared_gate.shape[1]), bf),
            dma((9,)),
            dma((2,)),
            dma((3,)),
            dma((3,)),
        ]
        + [dma(pairs)] * 4
        + [dma((depth, TILES))] * 6
        + [dma(pairs)] * 2
        + [dma((3,))] * 2
        + [dma((4,))] * 2,
        compiler_params=pltpu.CompilerParams(
            collective_id=0, has_side_effects=True, vmem_limit_bytes=56 * 1024 * 1024
        ),
        cost_estimate=pl.CostEstimate(flops=flops * 2, bytes_accessed=40_000_000, transcendentals=0),
    )(
        normed,
        weights,
        expert_gate,
        expert_up,
        expert_down,
        shared_gate,
        shared_up,
        shared_down,
        value,
        cgate,
        cweight,
        taps,
        gain.reshape(1, -1),
        shift.reshape(1, -1),
    )


def moe_general(normed, routes, route_weights, expert_gate, expert_up, expert_down, shared_gate, shared_up, shared_down):
    rows_b, per_row = routes.shape
    model_width = normed.shape[1]
    groups = lax.axis_size("ep")
    capacity = 2 * rows_b * per_row // groups
    flat_expert = routes.reshape(-1)
    owner_row = jnp.arange(rows_b * per_row, dtype=jnp.int32) // per_row
    expert_hits = (flat_expert[:, None] == jnp.arange(groups, dtype=jnp.int32)[None, :]).astype(
        jnp.int32
    )
    slot_rank = jnp.sum((jnp.cumsum(expert_hits, axis=0) - expert_hits) * expert_hits, axis=1)
    slot_index = flat_expert * capacity + slot_rank
    outgoing = (
        jnp.zeros((groups * capacity, model_width), jnp.bfloat16)
        .at[slot_index]
        .set(normed[owner_row])
    )
    outgoing = outgoing.reshape(groups, capacity, model_width)
    slot_share = capacity // lax.axis_size("tp")
    own_slots = lax.dynamic_slice_in_dim(outgoing, lax.axis_index("tp") * slot_share, slot_share, 1)
    partial_rows = lax.all_to_all(own_slots, "ep", split_axis=0, concat_axis=0, tiled=True)
    arrived = lax.all_gather(partial_rows, "tp", axis=1, tiled=True)
    arrived_rows = arrived.reshape(groups * capacity, model_width)
    gate_value = jnp.dot(arrived_rows, expert_gate[0], preferred_element_type=jnp.float32)
    upward = jnp.dot(arrived_rows, expert_up[0], preferred_element_type=jnp.float32)
    expert_hidden = (jax.nn.silu(gate_value) * upward).astype(jnp.bfloat16)
    shared_hidden = (
        jax.nn.silu(jnp.dot(normed, shared_gate, preferred_element_type=jnp.float32))
        * jnp.dot(normed, shared_up, preferred_element_type=jnp.float32)
    ).astype(jnp.bfloat16)
    columns = expert_down.shape[2]
    routed_sum = jnp.dot(
        lax.all_gather(expert_hidden, "tp", axis=1, tiled=True),
        expert_down[0],
        preferred_element_type=jnp.float32,
    )
    shared_sum = jnp.dot(
        lax.all_gather(shared_hidden, "tp", axis=1, tiled=True),
        shared_down,
        preferred_element_type=jnp.float32,
    )
    expert_out = routed_sum.astype(jnp.bfloat16).reshape(groups, capacity, columns)
    returned = lax.all_to_all(expert_out, "ep", split_axis=0, concat_axis=0, tiled=True).reshape(
        groups * capacity, columns
    )
    picked = returned[slot_index].astype(jnp.float32) * route_weights.reshape(-1)[:, None]
    moe_sum = jnp.sum(picked.reshape(rows_b, per_row, columns), axis=1) + shared_sum
    return moe_sum.astype(jnp.bfloat16)


def conv_general(conv_value, conv_gate, conv_taps, norm_gain, norm_shift, conv_out_weight):
    tap_count = conv_taps.shape[0]
    rows_a = conv_value.shape[0]
    glu_rows = (
        conv_value.astype(jnp.float32) * jax.nn.sigmoid(conv_gate.astype(jnp.float32))
    ).astype(jnp.bfloat16)
    before = from_behind(glu_rows[rows_a - (tap_count - 1) :], "ep", 1)
    padded = jnp.concatenate([before, glu_rows], axis=0)
    filtered = jnp.zeros(glu_rows.shape, jnp.float32)
    for offset in range(tap_count):
        filtered = filtered + conv_taps[offset] * padded[offset : offset + rows_a].astype(
            jnp.float32
        )
    row_total, squares = lax.psum(
        (jnp.sum(filtered, axis=1), jnp.sum(filtered * filtered, axis=1)), "tp"
    )
    channels = conv_out_weight.shape[0]
    row_mean = row_total / channels
    row_square = squares / channels
    scaled = (filtered - row_mean[:, None]) * lax.rsqrt(row_square - row_mean * row_mean + 1e-05)[
        :, None
    ]
    conv_hidden = jax.nn.silu(scaled * norm_gain + norm_shift).astype(jnp.bfloat16)
    conv_sum = jnp.dot(
        lax.all_gather(conv_hidden, "tp", axis=1, tiled=True),
        conv_out_weight,
        preferred_element_type=jnp.float32,
    )
    return conv_sum.astype(jnp.bfloat16)


def body(
    conv_value,
    conv_gate,
    conv_taps,
    norm_gain,
    norm_shift,
    conv_out_weight,
    moe_input,
    moe_gain,
    routes,
    route_weights,
    expert_gate,
    expert_up,
    expert_down,
    shared_gate,
    shared_up,
    shared_down,
):
    inputs = moe_input.astype(jnp.float32)
    normed = (
        inputs * lax.rsqrt(jnp.mean(inputs * inputs, axis=1, keepdims=True) + 1e-06) * moe_gain
    ).astype(jnp.bfloat16)
    conv = (conv_value, conv_gate, conv_taps, norm_gain, norm_shift, conv_out_weight)
    moe = (routes, route_weights, expert_gate, expert_up, expert_down, shared_gate, shared_up, shared_down)
    if lax.axis_size("tp") == 4 and lax.axis_size("ep") in (2, 4, 8):
        return fused(conv, normed, *moe)
    return (conv_general(*conv), moe_general(normed, *moe))


def solution(mesh):
    return jax.shard_map(
        body,
        mesh=mesh,
        in_specs=(
            P("ep", "tp"),
            P("ep", "tp"),
            P(None, "tp"),
            P("tp"),
            P("tp"),
            P(None, "tp"),
            P("ep", None),
            P(),
            P("ep", None),
            P("ep", None),
            P("ep", None, "tp"),
            P("ep", None, "tp"),
            P("ep", None, "tp"),
            P(None, "tp"),
            P(None, "tp"),
            P(None, "tp"),
        ),
        out_specs=(P("ep", "tp"), P("ep", "tp")),
        check_vma=False,
    )
```

profile of v0, /device:TPU:10, one launch (start us, length us, event | category | flops | bytes accessed | tf_op | source)
XLA Modules:
  0.0 103.2 jit_solution(15464607529236591176)
XLA Ops:
  0.7 0.1 stack.35
  0.8 1.2 %fusion = f32[128]{0:T(128)S(1)} fusion(bf16[128,2048]{1,0:T(8,128)(2,1)} %param.22), kind=kLoop, calls=%fused_computation.2 | loop fusion | flops 786304 | bytes 524800 | tf_op jit(solution)/shard_map/reduce_sum | solution.py:537
  2.1 0.8 select_reduce_fusion
  2.8 0.7 copy.20.weights
  3.6 2.0 %fusion.2.normed = bf16[128,2048]{1,0:T(8,128)(2,1)} fusion(bf16[128,2048]{1,0:T(8,128)(2,1)} %param.22, f32[2048]{0:T(1024)} %param.23, f32[128]{0:T(128)S(1)} %add_rsqrt_fusion), kind=kLoop, calls=%fused_computation.4 | loop fusion | flops 1048576 | bytes 1057280 | tf_op jit(solution)/shard_map/convert_element_type | solution.py:538
  5.6 94.1 %shard_map.167 = (bf16[512,512]{1,0:T(8,128)(2,1)}, bf16[128,512]{1,0:T(8,128)(2,1)}) custom-call(bf16[128,2048]{1,0:T(8,128)(2,1)} %fusion.2.normed, f32[128,8]{1,0:T(8,128)} %copy.20.weights, bf16[1,2048,1024]{2,1,0:T(8,128)(2,1)} %gate_hbm.1, bf16[1,2048,1024]{2,1,0:T(8,128)(2,1)} %up_hbm.1, bf16[1,4096,512]{2,1,0:T(8,128)(2,1)} %down_hbm.1, ...), custom_call_target="tpu_custom_call" | custom-call | flops 25769803776 | bytes 40000000 | tf_op jit(solution)/shard_map/pallas_call | solution.py:374
  99.8 1.9 %copy.23 = bf16[512,512]{1,0:T(8,128)(2,1)} copy(bf16[512,512]{1,0:T(8,128)(2,1)} %get-tuple-element.4) | data formatting | bytes 1048576
  101.6 1.6 %copy.24 = bf16[128,512]{1,0:T(8,128)(2,1)} copy(bf16[128,512]{1,0:T(8,128)(2,1)} %get-tuple-element.5) | data formatting | bytes 262144
  (1 shorter events, 0.0 us)
where the time goes:
time: 103 us
  Pallas kernels  94.1 us (91%)
  local copies, waits for them, and re-layouts  4.25 us (4%)
  other arithmetic  4.04 us (4%)
    pallas_call x1, Pallas kernels, fused(): pl.pallas_call(functools.partial(moe_kernel, depth), out_shape=(jax.Shape...  94.1 us
    unnamed x2, local copies, waits for them, and re-layouts  3.44 us

commit v1 on v0

v1 whole, which is shorter than its diff:
```python
import functools
import types

import jax
import jax.numpy as jnp
from jax import lax
from jax.experimental import pallas as pl
from jax.experimental.pallas import tpu as pltpu
from jax.sharding import PartitionSpec as P

MESH = pl.DeviceIdType.MESH
CHUNK = 64
SPAN = 128
PIECES = 4
TP = 4


def from_behind(value, axis, steps):
    count = lax.axis_size(axis)
    initial, last = (max(0, -steps), min(count, count - steps))
    return lax.ppermute(value, axis, [(source, source + steps) for source in range(initial, last)])


def silu(v):
    return v / (1.0 + jnp.exp(-v))


def phase(step):
    def run(*args, **settings):
        with jax.named_scope(step.__name__):
            return step(*args, **settings)

    return run


def layer_kernel(depth, names, *refs):
    r = types.SimpleNamespace(**dict(zip(names, refs, strict=True)))
    e = lax.axis_index("ep")
    q = lax.axis_index("tp")
    z, x = e // 2, e % 2
    y, c = q // 2, q % 2
    side = y * 2 + (1 - c)
    far = (1 - y) * 2 + c
    opposite = (1 - y) * 2 + (1 - c)
    sister, across, beside = (e, side), (e, far), (z * 2 + (1 - x), q)
    blocks = 2 * depth
    bf, f32 = jnp.bfloat16, jnp.float32

    tokens, hidden, chidden, shidden, padded = r.tokens, r.hidden, r.chidden, r.shidden, r.padded
    rows, width = r.x_in.shape
    half = width // 2
    units = r.gate.shape[1]
    rows_a, channels = r.value.shape
    tap_count, edge = r.taps.shape[0], r.halo.shape[0]
    lead = edge - (tap_count - 1)
    chunks = rows_a // CHUNK
    spans = rows_a // SPAN
    everything = slice(0, rows)

    upper = z // 2
    inside = (z + upper) % 2
    inner, outer = inside == 1, inside == 0
    mate = z + 1 - 2 * (z % 2)
    facing = depth - 1 - z
    origin = [z, mate, 2 - upper, 3 - 3 * upper]
    back = [0, 1, 3 - inside, 3 - inside]

    def place(b):
        return origin[b // 2] * 2 + (x if b % 2 == 0 else 1 - x)

    def slab(size, parts, i):
        return slice(i * size // parts, (i + 1) * size // parts)

    def dot(a, b):
        return jnp.dot(a, b, preferred_element_type=f32)

    def copy(src, dst, send, recv, device):
        return pltpu.make_async_remote_copy(
            src_ref=src, dst_ref=dst, send_sem=send.at[0], recv_sem=recv, device_id=device, device_id_type=MESH
        )

    def launch(*args):
        copy(*args).start()

    def landed(like, recv):
        copy(like, like, r.e_send, recv, beside).wait_recv()

    def gone(like, send):
        copy(like, like, send, r.e_recv.at[0], beside).wait_send()

    loads = []

    def load(*pairs):
        sem = r.load_sem.at[len(loads)]
        loads.append(sem)
        for src, dst in pairs:
            pltpu.make_async_copy(src, dst, sem).start()
        return sem

    def loaded(sem, src, dst):
        pltpu.make_async_copy(src, dst, sem).wait()

    gate_cols = [slab(units, PIECES, t) for t in range(PIECES)]
    tail_rows, other_rows = slice(rows_a - CHUNK, rows_a), slice(0, rows_a - CHUNK)
    x_sem = load((r.x_hbm, r.x_in))
    moe_gain_sem = load((r.moe_gain_hbm, r.moe_gain))
    tail_sems = [
        load((r.value_hbm.at[tail_rows], r.value.at[tail_rows])),
        load((r.cgate_hbm.at[tail_rows], r.cgate.at[tail_rows])),
    ]
    gate_sems = [
        load((r.gate_hbm.at[0, :, cols], r.gate.at[:, cols]), (r.up_hbm.at[0, :, cols], r.up.at[:, cols]))
        for cols in gate_cols
    ]
    rest = [
        (r.value_hbm.at[other_rows], r.value.at[other_rows]),
        (r.cgate_hbm.at[other_rows], r.cgate.at[other_rows]),
        (r.sgate_hbm, r.sgate),
        (r.sup_hbm, r.sup),
        (r.taps_hbm, r.taps),
        (r.gain_hbm, r.gain),
        (r.shift_hbm, r.shift),
        (r.routes_hbm, r.routes),
        (r.route_weights_hbm, r.route_weights),
    ]
    rest_sems = [load(pair) for pair in rest]

    peers = [(place(b), q) for b in range(1, blocks)]
    peers += [(e, (q + k) % TP) for k in range(1, TP)]
    barrier = pltpu.get_barrier_semaphore()
    for peer in peers:
        pl.semaphore_signal(barrier, inc=1, device_id=peer, device_id_type=MESH)

    def chunk_of(i):
        return pl.multiple_of(i * CHUNK, CHUNK)

    def glu(i, carry):
        at = pl.ds(chunk_of(i), CHUNK)
        gated = r.value[at, :].astype(f32) * (1.0 / (1.0 + jnp.exp(-r.cgate[at, :].astype(f32))))
        padded[pl.ds(pl.multiple_of(i * CHUNK + edge, 8), CHUNK), :] = gated.astype(bf).astype(f32)
        return carry

    lane = lax.broadcasted_iota(jnp.int32, (CHUNK, 128), 1)

    def convolve(i, carry):
        start = chunk_of(i)
        at = pl.ds(start, CHUNK)
        sums, squares = jnp.zeros((CHUNK, 128), f32), jnp.zeros((CHUNK, 128), f32)
        for column in range(0, channels, 128):
            cols = slice(column, column + 128)
            window = padded[pl.ds(start, CHUNK + edge), cols]
            total = jnp.zeros((CHUNK, 128), f32)
            for b in range(8):
                size = CHUNK + (8 if b else 0)
                part = None
                for a in range(edge // 8 + 1):
                    j = 8 * a + b - lead
                    if 0 <= j < tap_count:
                        term = r.taps[j : j + 1, cols] * window[8 * a : 8 * a + size]
                        part = term if part is None else part + term
                if b:
                    part = pltpu.roll(part, size - b, 0)[:CHUNK]
                total = total + part
            r.filtered[at, cols] = total
            sums = sums + total
            squares = squares + total * total
        row_sum = jnp.sum(sums, axis=1, keepdims=True)
        row_squares = jnp.sum(squares, axis=1, keepdims=True)
        r.stats[at, :] = jnp.where(lane == 0, row_sum, jnp.where(lane == 1, row_squares, 0.0))
        return carry

    @phase
    def conv(first_chunk, last_chunk):
        lax.fori_loop(first_chunk, last_chunk, convolve, 0)

    @phase
    def halo():
        landed(r.halo, r.e_recv.at[0])
        padded[0:edge, :] = jnp.where(e == 0, 0.0, r.halo[...].astype(f32))

    @phase
    def send_stats():
        turned = r.stats[...].T
        lines = [turned[k : k + 1, slab(rows_a, spans, j)] for k in range(2) for j in range(spans)]
        r.rowsums[q] = jnp.concatenate(lines, axis=0)
        mine = r.rowsums.at[q]
        for k in range(1, TP):
            launch(mine, mine, r.m_send, r.m_recv.at[0], (e, (q + k) % TP))

    @phase
    def normalise():
        landed(r.rowsums.at[0 : TP - 1], r.m_recv.at[0])
        whole = (r.rowsums[0] + r.rowsums[1] + r.rowsums[2] + r.rowsums[3]) / (channels * TP)
        turned = jnp.concatenate([whole, jnp.zeros((SPAN - 2 * spans, SPAN), f32)], axis=0).T
        r.stats[0:SPAN, :] = turned
        for j in range(spans):

            def scale(i, carry):
                here = chunk_of(i)
                at = pl.ds(pl.multiple_of(here + j * SPAN, CHUNK), CHUNK)
                both = r.stats[pl.ds(here, CHUNK), :]
                mean, square = both[:, j : j + 1], both[:, spans + j : spans + j + 1]
                scaled = (r.filtered[at, :] - mean) * lax.rsqrt(square - mean * mean + 1e-05)
                chidden[q, at, :] = silu(scaled * r.gain[...] + r.shift[...]).astype(bf)
                return carry

            lax.fori_loop(0, SPAN // CHUNK, scale, 0)

    def send_conv(j):
        block = chidden.at[q, slab(rows_a, spans, j)]
        launch(block, block, r.c_send, r.ca_recv.at[j], across)
        launch(block, block, r.c_send, r.cs_recv.at[0], sister)

    @phase
    def relay_conv(j):
        block = chidden.at[far, slab(rows_a, spans, j)]
        landed(block, r.ca_recv.at[j])
        launch(block, block, r.c_send, r.cf_recv.at[j], sister)

    def conv_part(j, k):
        at = pl.ds(pl.multiple_of(k * channels, channels), channels)
        return dot(chidden[k, slab(rows_a, spans, j), :], r.cweight[at, :])

    @phase
    def project(j, base=None):
        at = slab(rows_a, spans, j)
        total = conv_part(j, q) + conv_part(j, side) + conv_part(j, far) if base is None else base + conv_part(j, far)
        landed(chidden.at[opposite, at], r.cf_recv.at[j])
        r.conv_done[at, :] = (total + conv_part(j, opposite)).astype(bf)
        pltpu.make_async_copy(r.conv_done.at[at], r.conv_out.at[at], out_sem).start()

    def towards(src, slot, z_to):
        return copy(src, tokens.at[2 * slot, c], r.z_send, r.z_recv.at[slot - 1], (z_to * 2 + x, q))

    halves = [slab(rows, 2, i) for i in range(2)]

    @phase
    def pass_on(b, i=0, part=everything, condition=None):
        block = tokens.at[b, c, part]

        def along():
            (towards(block, 3, facing) if b == 2 else towards(block, b // 2, mate)).start()

        def act():
            landed(block, r.z_recv.at[b // 2 - 1] if b % 2 == 0 else r.t_recv.at[b // 2 + (1 if b > 1 else i)])
            if b % 2 == 0:
                if condition is inner:
                    along()
                elif condition is None:
                    pl.when(inner)(along)
                launch(block, tokens.at[b + 1, c, part], r.t_send, r.t_recv.at[b // 2 + 1], beside)
            launch(block, block, r.f_send, r.f_recv.at[b if b > 1 else i], sister)

        if condition is None:
            act()
        else:
            pl.when(condition)(act)

    @phase
    def swap_wait(b, i=0, part=everything):
        landed(tokens.at[b, 1 - c, part], r.f_recv.at[b if b > 1 else i])

    @phase
    def first(b, part, cols):
        def product(weight):
            return sum(dot(tokens[b, h, part, :], weight[h * half : (h + 1) * half, cols]) for h in range(2))

        hidden[b, q, part, cols] = (silu(product(r.gate)) * product(r.up)).astype(bf)
        block = hidden.at[b, q, part, cols]
        launch(block, block, r.h_send, r.y_recv.at[b], across)
        launch(block, block, r.h_send, r.p_recv.at[b], sister)

    def block_first(b):
        for t in range(2):
            first(b, everything, slab(units, 2, t))

    @phase
    def relay(b):
        block = hidden.at[b, far]
        landed(block, r.y_recv.at[b])
        launch(block, block, r.h_send, r.p_recv.at[b], sister)

    @phase
    def second_wait(b):
        landed(hidden.at[b, 0:2], r.p_recv.at[b])

    @phase
    def second(b):
        total = sum(dot(hidden[b, k], r.down[k * units : (k + 1) * units, :]) for k in range(TP))
        if b == 0:
            r.returned[0] = total.astype(bf)
        else:
            r.outgoing[b] = total.astype(bf)
            there = 2 * back[b // 2] + b % 2
            launch(r.outgoing.at[b], r.returned.at[there], r.r_send, r.r_recv.at[0], (place(b), q))

    def finish(b):
        second_wait(b)
        second(b)

    @phase
    def norm():
        loaded(x_sem, r.x_hbm, r.x_in)
        loaded(moe_gain_sem, r.moe_gain_hbm, r.moe_gain)
        for i in range(rows // 16):
            at = slice(i * 16, i * 16 + 16)
            v = r.x_in[at, :].astype(f32)
            scale = lax.rsqrt(jnp.mean(v * v, axis=1, keepdims=True) + 1e-06)
            normed = (v * scale * r.moe_gain[...]).astype(bf)
            tokens[0, 0, at, :] = normed[:, :half]
            tokens[0, 1, at, :] = normed[:, half:]

    @phase
    def tail_glu():
        loaded(tail_sems[0], r.value_hbm.at[tail_rows], r.value.at[tail_rows])
        loaded(tail_sems[1], r.cgate_hbm.at[tail_rows], r.cgate.at[tail_rows])
        glu(chunks - 1, 0)
        r.tail[...] = padded[rows_a:, :].astype(bf)

    @phase
    def meet():
        pl.semaphore_wait(barrier, len(peers))

    norm()
    tail_glu()
    meet()
    for i, part in enumerate(halves):
        launch(tokens.at[0, c, part], tokens.at[1, c, part], r.t_send, r.t_recv.at[i], beside)
    towards(tokens.at[0, c], 1, mate).start()
    pl.when(inner)(lambda: towards(tokens.at[0, c], 2, facing).start())
    launch(r.tail, r.halo, r.e_send, r.e_recv.at[0], ((e + 1) % blocks, q))

    for t, cols in enumerate(gate_cols):
        both = slab(units, PIECES // 2, 0)
        loaded(gate_sems[t], r.gate_hbm.at[0, :, both], r.gate.at[:, both])
        first(0, everything, cols)

    cweight_sem = load((r.cweight_hbm, r.cweight))
    down_sem = load((r.down_hbm.at[0], r.down))
    sdown_sem = load((r.sdown_hbm, r.sdown))
    out_sem = r.load_sem.at[len(loads)]

    @phase
    def glu_rest():
        for sem, pair in zip(rest_sems, rest, strict=True):
            loaded(sem, *pair)
        lax.fori_loop(0, chunks - 1, glu, 0)

    @phase
    def shared():
        def product(weight):
            return sum(dot(tokens[0, h], weight[h * half : (h + 1) * half, :]) for h in range(2))

        shidden[q] = (silu(product(r.sgate)) * product(r.sup)).astype(bf)
        launch(shidden.at[q], shidden.at[q], r.s_send, r.s_recv.at[0], across)
        launch(shidden.at[q], shidden.at[q], r.s_send, r.s_recv.at[1], sister)

    @phase
    def relay_shared():
        landed(shidden.at[far], r.s_recv.at[0])
        launch(shidden.at[far], shidden.at[far], r.s_send, r.s_recv.at[1], sister)

    @phase
    def shared_down():
        loaded(sdown_sem, r.sdown_hbm, r.sdown)
        landed(shidden.at[0:2], r.s_recv.at[1])
        share = shidden.shape[2]
        r.shared_sum[...] = sum(dot(shidden[k], r.sdown[k * share : (k + 1) * share, :]) for k in range(TP))

    @phase
    def combine():
        landed(r.returned.at[1:blocks], r.r_recv.at[0])
        routes, route_weights = r.routes[...], r.route_weights[...]
        lines = []
        for b in range(blocks):
            lines.append(jnp.sum(jnp.where(routes == place(b), route_weights, 0.0), axis=0, keepdims=True))
        lines.append(jnp.zeros((128 - blocks, rows), f32))
        weights = jnp.concatenate(lines, axis=0).T
        moe_sum = r.shared_sum[...]
        for b in range(blocks):
            moe_sum = moe_sum + weights[:, b : b + 1] * r.returned[b].astype(f32)
        r.done[...] = moe_sum.astype(bf)
        pltpu.make_async_copy(r.done, r.out, x_sem).start()

    glu_rest()
    shared()
    conv(1, 4)
    pass_on(1, 0, halves[0])
    conv(4, 5)
    swap_wait(1, 0, halves[0])
    for t in range(2):
        first(1, halves[0], slab(units, 2, t))
    pass_on(1, 1, halves[1])
    pass_on(2)
    pass_on(4, condition=inner)
    conv(5, 6)
    swap_wait(1, 1, halves[1])
    for t in range(2):
        first(1, halves[1], slab(units, 2, t))
    swap_wait(2)
    block_first(2)
    relay(0)
    conv(6, 7)
    pass_on(4, condition=outer)
    conv(7, chunks)
    halo()
    conv(0, 1)
    send_stats()
    pass_on(6, condition=inner)
    pass_on(3)
    swap_wait(4)
    block_first(4)
    relay(1)
    relay_shared()
    loaded(down_sem, r.down_hbm.at[0], r.down)
    finish(0)
    pass_on(6, condition=outer)
    pass_on(5)
    swap_wait(6)
    block_first(6)
    relay(2)
    finish(1)
    swap_wait(5)
    block_first(5)
    finish(2)
    normalise()
    pass_on(7)
    swap_wait(7)
    block_first(7)
    swap_wait(3)
    block_first(3)
    for j in range(spans):
        send_conv(j)
    for b in (4, 6, 5, 7, 3):
        relay(b)
        if b == 3:
            shared_down()
        finish(b)
    loaded(cweight_sem, r.cweight_hbm, r.cweight)
    landed(chidden.at[side], r.cs_recv.at[0])
    last = spans - 1
    for j in range(last):
        relay_conv(j)
        if j:
            project(j - 1)
    combine()
    r.partial[...] = conv_part(last, q) + conv_part(last, side)
    project(last - 1)
    relay_conv(last)
    project(last, r.partial[...])

    @phase
    def drain():
        gone(hidden.at[:, 0:3], r.h_send)
        gone(r.outgoing.at[1:blocks], r.r_send)
        gone(tokens.at[0:depth, c], r.t_send)
        gone(tokens.at[1:blocks, c], r.f_send)
        pl.when(inner)(lambda: gone(tokens.at[0:5, c], r.z_send))
        pl.when(outer)(lambda: gone(tokens.at[0, c], r.z_send))
        gone(r.rowsums.at[0 : TP - 1], r.m_send)
        gone(shidden.at[0:3], r.s_send)
        gone(chidden.at[0:3], r.c_send)
        gone(r.tail, r.e_send)
        pltpu.make_async_copy(r.done, r.out, x_sem).wait()
        pltpu.make_async_copy(r.conv_done, r.conv_out, out_sem).wait()

    drain()


def hand_out(conv_done, done, conv_out, out, conv_held, held, sems):
    parts = [(conv_done, conv_held, conv_out, slice(at, at + SPAN)) for at in range(0, conv_done.shape[0], SPAN)]
    parts.append((done, held, out, slice(0, done.shape[0])))
    ins = [pltpu.make_async_copy(src.at[at], mid.at[at], sems.at[0, i]) for i, (src, mid, _, at) in enumerate(parts)]
    outs = [pltpu.make_async_copy(mid.at[at], dst.at[at], sems.at[1, i]) for i, (_, mid, dst, at) in enumerate(parts)]
    for cp in ins:
        cp.start()
    for cp, then in zip(ins, outs):
        cp.wait()
        then.start()
    for cp in outs:
        cp.wait()


def fused(
    conv, moe_input, moe_gain, routes, route_weights, expert_gate, expert_up, expert_down, shared_gate, shared_up, shared_down
):
    value, cgate, taps, gain, shift, cweight = conv
    rows_a, channels = value.shape
    spans = rows_a // SPAN
    edge = -(-(taps.shape[0] - 1) // 8) * 8
    rows, width = moe_input.shape
    depth = lax.axis_size("ep") // 2
    blocks = 2 * depth
    units, columns = expert_gate.shape[2], expert_down.shape[2]
    bf, f32 = jnp.bfloat16, jnp.float32
    hbm = pl.BlockSpec(memory_space=pl.ANY)

    def held(like):
        return pltpu.VMEM(like.shape, like.dtype)

    def dma(*shape):
        return pltpu.SemaphoreType.DMA(shape)

    gain, shift, moe_gain = gain.reshape(1, -1), shift.reshape(1, -1), moe_gain.reshape(1, -1)
    routes, route_weights = routes.T, route_weights.T
    operands = dict(
        x_hbm=moe_input,
        gate_hbm=expert_gate,
        up_hbm=expert_up,
        down_hbm=expert_down,
        sgate_hbm=shared_gate,
        sup_hbm=shared_up,
        sdown_hbm=shared_down,
        value_hbm=value,
        cgate_hbm=cgate,
        cweight_hbm=cweight,
        taps_hbm=taps,
        gain_hbm=gain,
        shift_hbm=shift,
        moe_gain_hbm=moe_gain,
        routes_hbm=routes,
        route_weights_hbm=route_weights,
    )
    outputs = dict(
        conv_out=jax.ShapeDtypeStruct((rows_a, cweight.shape[1]), bf),
        out=jax.ShapeDtypeStruct((rows, columns), bf),
    )
    scratch = dict(
        x_in=held(moe_input),
        sgate=held(shared_gate),
        sup=held(shared_up),
        sdown=held(shared_down),
        value=held(value),
        cgate=held(cgate),
        cweight=held(cweight),
        taps=held(taps),
        gain=held(gain),
        shift=held(shift),
        moe_gain=held(moe_gain),
        routes=held(routes),
        route_weights=held(route_weights),
        gate=pltpu.VMEM(expert_gate.shape[1:], bf),
        up=pltpu.VMEM(expert_up.shape[1:], bf),
        down=pltpu.VMEM(expert_down.shape[1:], bf),
        padded=pltpu.VMEM((rows_a + edge, channels), f32),
        filtered=pltpu.VMEM((rows_a, channels), f32),
        stats=pltpu.VMEM((rows_a, 128), f32),
        tail=pltpu.VMEM((edge, channels), bf),
        halo=pltpu.VMEM((edge, channels), bf),
        rowsums=pltpu.VMEM((TP, 2 * spans, SPAN), f32),
        chidden=pltpu.VMEM((TP, rows_a, channels), bf),
        partial=pltpu.VMEM((SPAN, cweight.shape[1]), f32),
        tokens=pltpu.VMEM((blocks, 2, rows, width // 2), bf),
        hidden=pltpu.VMEM((blocks, TP, rows, units), bf),
        returned=pltpu.VMEM((blocks, rows, columns), bf),
        outgoing=pltpu.VMEM((blocks, rows, columns), bf),
        shidden=pltpu.VMEM((TP, rows, shared_gate.shape[1]), bf),
        shared_sum=pltpu.VMEM((rows, columns), f32),
        conv_done=held(outputs["conv_out"]),
        done=held(outputs["out"]),
        load_sem=dma(PIECES + 17),
        e_send=dma(1),
        e_recv=dma(1),
        t_send=dma(1),
        t_recv=dma(depth + 1),
        f_send=dma(1),
        f_recv=dma(blocks),
        z_send=dma(1),
        z_recv=dma(depth - 1),
        h_send=dma(1),
        y_recv=dma(blocks),
        p_recv=dma(blocks),
        r_send=dma(1),
        r_recv=dma(1),
        m_send=dma(1),
        m_recv=dma(1),
        s_send=dma(1),
        s_recv=dma(2),
        c_send=dma(1),
        ca_recv=dma(spans),
        cs_recv=dma(1),
        cf_recv=dma(spans),
    )
    flops = 2 * blocks * rows * (2 * width * units + 4 * units * columns)
    results = pl.pallas_call(
        functools.partial(layer_kernel, depth, (*operands, *outputs, *scratch)),
        out_shape=tuple(outputs.values()),
        in_specs=[hbm] * len(operands),
        out_specs=(hbm, hbm),
        scratch_shapes=list(scratch.values()),
        compiler_params=pltpu.CompilerParams(
            collective_id=0, has_side_effects=True, vmem_limit_bytes=56 * 1024 * 1024
        ),
        cost_estimate=pl.CostEstimate(flops=flops * 2, bytes_accessed=40_000_000, transcendentals=0),
    )(*operands.values())
    return pl.pallas_call(
        hand_out,
        out_shape=tuple(outputs.values()),
        in_specs=[hbm, hbm],
        out_specs=(hbm, hbm),
        scratch_shapes=[held(out) for out in outputs.values()] + [dma(2, spans + 1)],
        compiler_params=pltpu.CompilerParams(vmem_limit_bytes=56 * 1024 * 1024),
    )(*results)


def moe_general(normed, routes, route_weights, expert_gate, expert_up, expert_down, shared_gate, shared_up, shared_down):
    rows_b, per_row = routes.shape
    model_width = normed.shape[1]
    groups = lax.axis_size("ep")
    capacity = 2 * rows_b * per_row // groups
    flat_expert = routes.reshape(-1)
    owner_row = jnp.arange(rows_b * per_row, dtype=jnp.int32) // per_row
    expert_hits = (flat_expert[:, None] == jnp.arange(groups, dtype=jnp.int32)[None, :]).astype(
        jnp.int32
    )
    slot_rank = jnp.sum((jnp.cumsum(expert_hits, axis=0) - expert_hits) * expert_hits, axis=1)
    slot_index = flat_expert * capacity + slot_rank
    outgoing = (
        jnp.zeros((groups * capacity, model_width), jnp.bfloat16)
        .at[slot_index]
        .set(normed[owner_row])
    )
    outgoing = outgoing.reshape(groups, capacity, model_width)
    slot_share = capacity // lax.axis_size("tp")
    own_slots = lax.dynamic_slice_in_dim(outgoing, lax.axis_index("tp") * slot_share, slot_share, 1)
    partial_rows = lax.all_to_all(own_slots, "ep", split_axis=0, concat_axis=0, tiled=True)
    arrived = lax.all_gather(partial_rows, "tp", axis=1, tiled=True)
    arrived_rows = arrived.reshape(groups * capacity, model_width)
    gate_value = jnp.dot(arrived_rows, expert_gate[0], preferred_element_type=jnp.float32)
    upward = jnp.dot(arrived_rows, expert_up[0], preferred_element_type=jnp.float32)
    expert_hidden = (jax.nn.silu(gate_value) * upward).astype(jnp.bfloat16)
    shared_hidden = (
        jax.nn.silu(jnp.dot(normed, shared_gate, preferred_element_type=jnp.float32))
        * jnp.dot(normed, shared_up, preferred_element_type=jnp.float32)
    ).astype(jnp.bfloat16)
    columns = expert_down.shape[2]
    routed_sum = jnp.dot(
        lax.all_gather(expert_hidden, "tp", axis=1, tiled=True),
        expert_down[0],
        preferred_element_type=jnp.float32,
    )
    shared_sum = jnp.dot(
        lax.all_gather(shared_hidden, "tp", axis=1, tiled=True),
        shared_down,
        preferred_element_type=jnp.float32,
    )
    expert_out = routed_sum.astype(jnp.bfloat16).reshape(groups, capacity, columns)
    returned = lax.all_to_all(expert_out, "ep", split_axis=0, concat_axis=0, tiled=True).reshape(
        groups * capacity, columns
    )
    picked = returned[slot_index].astype(jnp.float32) * route_weights.reshape(-1)[:, None]
    moe_sum = jnp.sum(picked.reshape(rows_b, per_row, columns), axis=1) + shared_sum
    return moe_sum.astype(jnp.bfloat16)


def conv_general(conv_value, conv_gate, conv_taps, norm_gain, norm_shift, conv_out_weight):
    tap_count = conv_taps.shape[0]
    rows_a = conv_value.shape[0]
    glu_rows = (
        conv_value.astype(jnp.float32) * jax.nn.sigmoid(conv_gate.astype(jnp.float32))
    ).astype(jnp.bfloat16)
    before = from_behind(glu_rows[rows_a - (tap_count - 1) :], "ep", 1)
    padded = jnp.concatenate([before, glu_rows], axis=0)
    filtered = jnp.zeros(glu_rows.shape, jnp.float32)
    for offset in range(tap_count):
        filtered = filtered + conv_taps[offset] * padded[offset : offset + rows_a].astype(
            jnp.float32
        )
    row_total, squares = lax.psum(
        (jnp.sum(filtered, axis=1), jnp.sum(filtered * filtered, axis=1)), "tp"
    )
    channels = conv_out_weight.shape[0]
    row_mean = row_total / channels
    row_square = squares / channels
    scaled = (filtered - row_mean[:, None]) * lax.rsqrt(row_square - row_mean * row_mean + 1e-05)[
        :, None
    ]
    conv_hidden = jax.nn.silu(scaled * norm_gain + norm_shift).astype(jnp.bfloat16)
    conv_sum = jnp.dot(
        lax.all_gather(conv_hidden, "tp", axis=1, tiled=True),
        conv_out_weight,
        preferred_element_type=jnp.float32,
    )
    return conv_sum.astype(jnp.bfloat16)


def body(
    conv_value,
    conv_gate,
    conv_taps,
    norm_gain,
    norm_shift,
    conv_out_weight,
    moe_input,
    moe_gain,
    routes,
    route_weights,
    expert_gate,
    expert_up,
    expert_down,
    shared_gate,
    shared_up,
    shared_down,
):
    conv = (conv_value, conv_gate, conv_taps, norm_gain, norm_shift, conv_out_weight)
    moe = (routes, route_weights, expert_gate, expert_up, expert_down, shared_gate, shared_up, shared_down)
    if lax.axis_size("tp") == TP and lax.axis_size("ep") == 8 and moe_input.shape[0] == 128:
        return fused(conv, moe_input, moe_gain, *moe)
    inputs = moe_input.astype(jnp.float32)
    normed = (
        inputs * lax.rsqrt(jnp.mean(inputs * inputs, axis=1, keepdims=True) + 1e-06) * moe_gain
    ).astype(jnp.bfloat16)
    return (conv_general(*conv), moe_general(normed, *moe))


def solution(mesh):
    return jax.shard_map(
        body,
        mesh=mesh,
        in_specs=(
            P("ep", "tp"),
            P("ep", "tp"),
            P(None, "tp"),
            P("tp"),
            P("tp"),
            P(None, "tp"),
            P("ep", None),
            P(),
            P("ep", None),
            P("ep", None),
            P("ep", None, "tp"),
            P("ep", None, "tp"),
            P("ep", None, "tp"),
            P(None, "tp"),
            P(None, "tp"),
            P(None, "tp"),
        ),
        out_specs=(P("ep", "tp"), P("ep", "tp")),
        check_vma=False,
    )
```

time: 103 us -> 71.8 us (0.70)
  the two profiles are of different devices: /device:TPU:10 before, /device:TPU:1 now
where the time goes in v1:
time: 71.8 us; the launch traced here: 71.6 us
  Pallas kernels  70.8 us (99%)
  between operations  0.83 us (1%)
    pallas_call x1, Pallas kernels, fused(): pl.pallas_call(functools.partial(layer_kernel, depth, (*operands, *output...  68.8 us
    pallas_call x1, Pallas kernels, fused(): pl.pallas_call(hand_out, out_shape=tuple(outputs.values()), in_specs=[hbm...  1.91 us

profile of v1, /device:TPU:1, one launch (start us, length us, event | category | flops | bytes accessed | tf_op | source)
XLA Modules:
  0.0 71.6 jit_solution(12894292082615297402)
XLA Ops:
  0.6 68.8 %shard_map.167 = (bf16[512,512]{1,0:T(8,128)(2,1)}, bf16[128,512]{1,0:T(8,128)(2,1)}) custom-call(bf16[128,2048]{1,0:T(8,128)(2,1)} %refs_0_.1, bf16[1,2048,1024]{2,1,0:T(8,128)(2,1)} %refs_1_.1, bf16[1,2048,1024]{2,1,0:T(8,128)(2,1)} %refs_2_.1, bf16[1,4096,512]{2,1,0:T(8,128)(2,1)} %refs_3_.1, bf16[2048,128]{1,0:T(8,128)(2,1)} %refs_4_.1, ...), custom_call_target="tpu_custom_call" | custom-call | flops 25769803776 | bytes 40000000 | tf_op jit(solution)/shard_map/pallas_call | solution.py:585
  69.5 1.9 %shard_map.168 = (bf16[512,512]{1,0:T(8,128)(2,1)}, bf16[128,512]{1,0:T(8,128)(2,1)}) custom-call(bf16[512,512]{1,0:T(8,128)(2,1)} %get-tuple-element.4.conv_done, bf16[128,512]{1,0:T(8,128)(2,1)} %get-tuple-element.5.done), custom_call_target="tpu_custom_call" | custom-call | tf_op jit(solution)/shard_map/pallas_call | solution.py:596

commit v2 on v1

--- a/solution.py
+++ b/solution.py
@@ -226,8 +226,7 @@
         at = slab(rows_a, spans, j)
         total = conv_part(j, q) + conv_part(j, side) + conv_part(j, far) if base is None else base + conv_part(j, far)
         landed(chidden.at[opposite, at], r.cf_recv.at[j])
-        r.conv_done[at, :] = (total + conv_part(j, opposite)).astype(bf)
-        pltpu.make_async_copy(r.conv_done.at[at], r.conv_out.at[at], out_sem).start()
+        r.conv_out[at, :] = (total + conv_part(j, opposite)).astype(bf)
 
     def towards(src, slot, z_to):
         return copy(src, tokens.at[2 * slot, c], r.z_send, r.z_recv.at[slot - 1], (z_to * 2 + x, q))
@@ -338,7 +337,6 @@
     cweight_sem = load((r.cweight_hbm, r.cweight))
     down_sem = load((r.down_hbm.at[0], r.down))
     sdown_sem = load((r.sdown_hbm, r.sdown))
-    out_sem = r.load_sem.at[len(loads)]
 
     @phase
     def glu_rest():
@@ -379,8 +377,7 @@
         moe_sum = r.shared_sum[...]
         for b in range(blocks):
             moe_sum = moe_sum + weights[:, b : b + 1] * r.returned[b].astype(f32)
-        r.done[...] = moe_sum.astype(bf)
-        pltpu.make_async_copy(r.done, r.out, x_sem).start()
+        r.out[...] = moe_sum.astype(bf)
 
     glu_rest()
     shared()
@@ -414,12 +411,14 @@
     relay_shared()
     loaded(down_sem, r.down_hbm.at[0], r.down)
     finish(0)
+    swap_wait(3)
+    block_first(3)
     pass_on(6, condition=outer)
     pass_on(5)
+    finish(1)
     swap_wait(6)
     block_first(6)
     relay(2)
-    finish(1)
     swap_wait(5)
     block_first(5)
     finish(2)
@@ -427,13 +426,11 @@
     pass_on(7)
     swap_wait(7)
     block_first(7)
-    swap_wait(3)
-    block_first(3)
     for j in range(spans):
         send_conv(j)
-    for b in (4, 6, 5, 7, 3):
+    for b in (4, 3, 6, 5, 7):
         relay(b)
-        if b == 3:
+        if b == 7:
             shared_down()
         finish(b)
     loaded(cweight_sem, r.cweight_hbm, r.cweight)
@@ -443,10 +440,10 @@
         relay_conv(j)
         if j:
             project(j - 1)
-    combine()
     r.partial[...] = conv_part(last, q) + conv_part(last, side)
     project(last - 1)
     relay_conv(last)
+    combine()
     project(last, r.partial[...])
 
     @phase
@@ -461,23 +458,17 @@
         gone(shidden.at[0:3], r.s_send)
         gone(chidden.at[0:3], r.c_send)
         gone(r.tail, r.e_send)
-        pltpu.make_async_copy(r.done, r.out, x_sem).wait()
-        pltpu.make_async_copy(r.conv_done, r.conv_out, out_sem).wait()
 
     drain()
 
 
-def hand_out(conv_done, done, conv_out, out, conv_held, held, sems):
-    parts = [(conv_done, conv_held, conv_out, slice(at, at + SPAN)) for at in range(0, conv_done.shape[0], SPAN)]
-    parts.append((done, held, out, slice(0, done.shape[0])))
-    ins = [pltpu.make_async_copy(src.at[at], mid.at[at], sems.at[0, i]) for i, (src, mid, _, at) in enumerate(parts)]
-    outs = [pltpu.make_async_copy(mid.at[at], dst.at[at], sems.at[1, i]) for i, (_, mid, dst, at) in enumerate(parts)]
-    for cp in ins:
+def hand_out(conv_done, done, conv_out, out, sems):
+    copies = [
+        pltpu.make_async_copy(src, dst, sems.at[i]) for i, (src, dst) in enumerate(((conv_done, conv_out), (done, out)))
+    ]
+    for cp in copies:
         cp.start()
-    for cp, then in zip(ins, outs):
-        cp.wait()
-        then.start()
-    for cp in outs:
+    for cp in copies:
         cp.wait()
 
 
@@ -494,6 +485,7 @@
     units, columns = expert_gate.shape[2], expert_down.shape[2]
     bf, f32 = jnp.bfloat16, jnp.float32
     hbm = pl.BlockSpec(memory_space=pl.ANY)
+    vmem = pl.BlockSpec(memory_space=pltpu.VMEM)
 
     def held(like):
         return pltpu.VMEM(like.shape, like.dtype)
@@ -556,9 +548,7 @@
         outgoing=pltpu.VMEM((blocks, rows, columns), bf),
         shidden=pltpu.VMEM((TP, rows, shared_gate.shape[1]), bf),
         shared_sum=pltpu.VMEM((rows, columns), f32),
-        conv_done=held(outputs["conv_out"]),
-        done=held(outputs["out"]),
-        load_sem=dma(PIECES + 17),
+        load_sem=dma(PIECES + 16),
         e_send=dma(1),
         e_recv=dma(1),
         t_send=dma(1),
@@ -584,22 +574,22 @@
     flops = 2 * blocks * rows * (2 * width * units + 4 * units * columns)
     results = pl.pallas_call(
         functools.partial(layer_kernel, depth, (*operands, *outputs, *scratch)),
-        out_shape=tuple(outputs.values()),
+        out_shape=tuple(pltpu.VMEM(out.shape, bf) for out in outputs.values()),
         in_specs=[hbm] * len(operands),
-        out_specs=(hbm, hbm),
+        out_specs=(vmem, vmem),
         scratch_shapes=list(scratch.values()),
         compiler_params=pltpu.CompilerParams(
-            collective_id=0, has_side_effects=True, vmem_limit_bytes=56 * 1024 * 1024
+            collective_id=0, has_side_effects=True, vmem_limit_bytes=58720256
         ),
         cost_estimate=pl.CostEstimate(flops=flops * 2, bytes_accessed=40_000_000, transcendentals=0),
     )(*operands.values())
     return pl.pallas_call(
         hand_out,
         out_shape=tuple(outputs.values()),
-        in_specs=[hbm, hbm],
+        in_specs=[vmem, vmem],
         out_specs=(hbm, hbm),
-        scratch_shapes=[held(out) for out in outputs.values()] + [dma(2, spans + 1)],
-        compiler_params=pltpu.CompilerParams(vmem_limit_bytes=56 * 1024 * 1024),
+        scratch_shapes=[dma(2)],
+        compiler_params=pltpu.CompilerParams(vmem_limit_bytes=4 * 1024 * 1024),
     )(*results)
 
 

time: 71.8 us -> 69.8 us (0.972)
  Pallas kernels: 70.8 us -> 68.8 us
    pallas_call x1, Pallas kernels: 1.91 us -> 0.85 us  [fused(): pl.pallas_call(hand_out, out_shape=tuple(outputs.values()), in_specs=[vme...]
    pallas_call x1, Pallas kernels: 68.8 us -> 68 us  [fused(): pl.pallas_call(functools.partial(layer_kernel, depth, (*operands, *output...]
where the time goes in v2:
time: 69.8 us; the launch traced here: 69.6 us
  Pallas kernels  68.8 us (99%)
  between operations  0.83 us (1%)
    pallas_call x1, Pallas kernels, fused(): pl.pallas_call(functools.partial(layer_kernel, depth, (*operands, *output...  68 us

profile of v2, /device:TPU:1, one launch (start us, length us, event | category | flops | bytes accessed | tf_op | source)
XLA Modules:
  0.0 69.6 jit_solution(1664124360255975870)
XLA Ops:
  0.6 68.0 %shard_map.167 = (bf16[512,512]{1,0:T(8,128)(2,1)S(1)}, bf16[128,512]{1,0:T(8,128)(2,1)S(1)}) custom-call(bf16[128,2048]{1,0:T(8,128)(2,1)} %refs_0_.1, bf16[1,2048,1024]{2,1,0:T(8,128)(2,1)} %refs_1_.1, bf16[1,2048,1024]{2,1,0:T(8,128)(2,1)} %refs_2_.1, bf16[1,4096,512]{2,1,0:T(8,128)(2,1)} %refs_3_.1, bf16[2048,128]{1,0:T(8,128)(2,1)} %refs_4_.1, ...), custom_call_target="tpu_custom_call" | custom-call | flops 25769803776 | bytes 40000000 | tf_op jit(solution)/shard_map/pallas_call | solution.py:575
  68.6 0.8 %shard_map.168 = (bf16[512,512]{1,0:T(8,128)(2,1)}, bf16[128,512]{1,0:T(8,128)(2,1)}) custom-call(bf16[512,512]{1,0:T(8,128)(2,1)S(1)} %get-tuple-element.4.conv_done, bf16[128,512]{1,0:T(8,128)(2,1)S(1)} %get-tuple-element.5.done), custom_call_target="tpu_custom_call" | custom-call | tf_op jit(solution)/shard_map/pallas_call | solution.py:586

commit v3 on v2

--- a/solution.py
+++ b/solution.py
@@ -51,7 +51,8 @@
     half = width // 2
     units = r.gate.shape[1]
     rows_a, channels = r.value.shape
-    tap_count, edge = r.taps.shape[0], r.halo.shape[0]
+    tap_count, edge = r.taps.shape[0], r.edges.shape[1]
+    tail_out, halo_rows, passing = (r.edges.at[i] for i in range(3))
     lead = edge - (tap_count - 1)
     chunks = rows_a // CHUNK
     spans = rows_a // SPAN
@@ -125,11 +126,15 @@
     ]
     rest_sems = [load(pair) for pair in rest]
 
-    peers = [(place(b), q) for b in range(1, blocks)]
-    peers += [(e, (q + k) % TP) for k in range(1, TP)]
+    peers = [beside, (mate * 2 + x, q)] + [(e, (q + k) % TP) for k in range(1, TP)]
     barrier = pltpu.get_barrier_semaphore()
+
+    def greet(peer):
+        pl.semaphore_signal(barrier, inc=1, device_id=peer, device_id_type=MESH)
+
     for peer in peers:
-        pl.semaphore_signal(barrier, inc=1, device_id=peer, device_id_type=MESH)
+        greet(peer)
+    pl.when(inner)(lambda: greet((facing * 2 + x, q)))
 
     def chunk_of(i):
         return pl.multiple_of(i * CHUNK, CHUNK)
@@ -175,8 +180,26 @@
 
     @phase
     def halo():
-        landed(r.halo, r.e_recv.at[0])
-        padded[0:edge, :] = jnp.where(e == 0, 0.0, r.halo[...].astype(f32))
+        @pl.when(e > 0)
+        def _():
+            landed(halo_rows, r.e_recv.at[0])
+            padded[0:edge, :] = halo_rows[...].astype(f32)
+
+        @pl.when(e == 0)
+        def _():
+            padded[0:edge, :] = jnp.zeros((edge, channels), f32)
+
+    onward = (x == 0) & (z < depth - 1)
+
+    @phase
+    def send_edge():
+        pl.when(x == 0)(lambda: launch(tail_out, halo_rows, r.e_send, r.e_recv.at[0], beside))
+        pl.when(x == 1)(lambda: launch(tail_out, passing, r.e_send, r.e_recv.at[1], beside))
+
+    @phase
+    def relay_edge():
+        pl.when(x == 0)(lambda: landed(passing, r.e_recv.at[1]))
+        pl.when(onward)(lambda: launch(passing, halo_rows, r.e_send, r.e_recv.at[0], ((z + 1) * 2 + x, q)))
 
     @phase
     def send_stats():
@@ -314,11 +337,12 @@
         loaded(tail_sems[0], r.value_hbm.at[tail_rows], r.value.at[tail_rows])
         loaded(tail_sems[1], r.cgate_hbm.at[tail_rows], r.cgate.at[tail_rows])
         glu(chunks - 1, 0)
-        r.tail[...] = padded[rows_a:, :].astype(bf)
+        tail_out[...] = padded[rows_a:, :].astype(bf)
 
     @phase
     def meet():
-        pl.semaphore_wait(barrier, len(peers))
+        pl.when(inner)(lambda: pl.semaphore_wait(barrier, len(peers) + 1))
+        pl.when(outer)(lambda: pl.semaphore_wait(barrier, len(peers)))
 
     norm()
     tail_glu()
@@ -327,7 +351,7 @@
         launch(tokens.at[0, c, part], tokens.at[1, c, part], r.t_send, r.t_recv.at[i], beside)
     towards(tokens.at[0, c], 1, mate).start()
     pl.when(inner)(lambda: towards(tokens.at[0, c], 2, facing).start())
-    launch(r.tail, r.halo, r.e_send, r.e_recv.at[0], ((e + 1) % blocks, q))
+    send_edge()
 
     for t, cols in enumerate(gate_cols):
         both = slab(units, PIECES // 2, 0)
@@ -390,6 +414,7 @@
     pass_on(1, 1, halves[1])
     pass_on(2)
     pass_on(4, condition=inner)
+    relay_edge()
     conv(5, 6)
     swap_wait(1, 1, halves[1])
     for t in range(2):
@@ -398,40 +423,46 @@
     block_first(2)
     relay(0)
     conv(6, 7)
-    pass_on(4, condition=outer)
-    conv(7, chunks)
-    halo()
-    conv(0, 1)
-    send_stats()
     pass_on(6, condition=inner)
     pass_on(3)
-    swap_wait(4)
-    block_first(4)
+    conv(7, chunks)
+    swap_wait(3)
+    block_first(3)
+    pass_on(4, condition=outer)
     relay(1)
     relay_shared()
     loaded(down_sem, r.down_hbm.at[0], r.down)
     finish(0)
-    swap_wait(3)
-    block_first(3)
+    swap_wait(4)
+    block_first(4)
+    halo()
+    conv(0, 1)
+    send_stats()
     pass_on(6, condition=outer)
     pass_on(5)
     finish(1)
     swap_wait(6)
     block_first(6)
     relay(2)
-    swap_wait(5)
-    block_first(5)
     finish(2)
+    relay(3)
+    finish(3)
     normalise()
+    send_conv(0)
+    relay(4)
+    finish(4)
     pass_on(7)
     swap_wait(7)
     block_first(7)
-    for j in range(spans):
+    relay(6)
+    finish(6)
+    swap_wait(5)
+    block_first(5)
+    for j in range(1, spans):
         send_conv(j)
-    for b in (4, 3, 6, 5, 7):
+    shared_down()
+    for b in (7, 5):
         relay(b)
-        if b == 7:
-            shared_down()
         finish(b)
     loaded(cweight_sem, r.cweight_hbm, r.cweight)
     landed(chidden.at[side], r.cs_recv.at[0])
@@ -457,7 +488,8 @@
         gone(r.rowsums.at[0 : TP - 1], r.m_send)
         gone(shidden.at[0:3], r.s_send)
         gone(chidden.at[0:3], r.c_send)
-        gone(r.tail, r.e_send)
+        pl.when(onward)(lambda: gone(r.edges.at[0:2], r.e_send))
+        pl.when(jnp.logical_not(onward))(lambda: gone(tail_out, r.e_send))
 
     drain()
 
@@ -537,8 +569,7 @@
         padded=pltpu.VMEM((rows_a + edge, channels), f32),
         filtered=pltpu.VMEM((rows_a, channels), f32),
         stats=pltpu.VMEM((rows_a, 128), f32),
-        tail=pltpu.VMEM((edge, channels), bf),
-        halo=pltpu.VMEM((edge, channels), bf),
+        edges=pltpu.VMEM((3, edge, channels), bf),
         rowsums=pltpu.VMEM((TP, 2 * spans, SPAN), f32),
         chidden=pltpu.VMEM((TP, rows_a, channels), bf),
         partial=pltpu.VMEM((SPAN, cweight.shape[1]), f32),
@@ -550,7 +581,7 @@
         shared_sum=pltpu.VMEM((rows, columns), f32),
         load_sem=dma(PIECES + 16),
         e_send=dma(1),
-        e_recv=dma(1),
+        e_recv=dma(2),
         t_send=dma(1),
         t_recv=dma(depth + 1),
         f_send=dma(1),

time: 69.8 us -> 67.7 us (0.970)
  Pallas kernels: 68.8 us -> 66.8 us
    pallas_call x1, Pallas kernels: 68 us -> 65.9 us  [fused(): pl.pallas_call(functools.partial(layer_kernel, depth, (*operands, *output...]
where the time goes in v3:
time: 67.7 us; the launch traced here: 67.6 us
  Pallas kernels  66.8 us (99%)
  between operations  0.81 us (1%)
    pallas_call x1, Pallas kernels, fused(): pl.pallas_call(functools.partial(layer_kernel, depth, (*operands, *output...  65.9 us

profile of v3, /device:TPU:1, one launch (start us, length us, event | category | flops | bytes accessed | tf_op | source)
XLA Modules:
  0.0 67.6 jit_solution(11777431516810775105)
XLA Ops:
  0.6 65.9 %shard_map.167 = (bf16[512,512]{1,0:T(8,128)(2,1)S(1)}, bf16[128,512]{1,0:T(8,128)(2,1)S(1)}) custom-call(bf16[128,2048]{1,0:T(8,128)(2,1)} %refs_0_.1, bf16[1,2048,1024]{2,1,0:T(8,128)(2,1)} %refs_1_.1, bf16[1,2048,1024]{2,1,0:T(8,128)(2,1)} %refs_2_.1, bf16[1,4096,512]{2,1,0:T(8,128)(2,1)} %refs_3_.1, bf16[2048,128]{1,0:T(8,128)(2,1)} %refs_4_.1, ...), custom_call_target="tpu_custom_call" | custom-call | flops 25769803776 | bytes 40000000 | tf_op jit(solution)/shard_map/pallas_call | solution.py:606
  66.6 0.8 %shard_map.168 = (bf16[512,512]{1,0:T(8,128)(2,1)}, bf16[128,512]{1,0:T(8,128)(2,1)}) custom-call(bf16[512,512]{1,0:T(8,128)(2,1)S(1)} %get-tuple-element.4.conv_done, bf16[128,512]{1,0:T(8,128)(2,1)S(1)} %get-tuple-element.5.done), custom_call_target="tpu_custom_call" | custom-call | tf_op jit(solution)/shard_map/pallas_call | solution.py:617

commit v4 on v3

--- a/solution.py
+++ b/solution.py
@@ -390,35 +390,41 @@
         r.shared_sum[...] = sum(dot(shidden[k], r.sdown[k * share : (k + 1) * share, :]) for k in range(TP))
 
     @phase
-    def combine():
-        landed(r.returned.at[1:blocks], r.r_recv.at[0])
+    def weigh():
         routes, route_weights = r.routes[...], r.route_weights[...]
         lines = []
         for b in range(blocks):
             lines.append(jnp.sum(jnp.where(routes == place(b), route_weights, 0.0), axis=0, keepdims=True))
         lines.append(jnp.zeros((128 - blocks, rows), f32))
-        weights = jnp.concatenate(lines, axis=0).T
+        r.weights[...] = jnp.concatenate(lines, axis=0).T
+        r.shared_sum[...] += r.weights[:, 0:1] * r.returned[0].astype(f32)
+
+    @phase
+    def combine():
+        landed(r.returned.at[1:blocks], r.r_recv.at[0])
+        weights = r.weights[...]
         moe_sum = r.shared_sum[...]
-        for b in range(blocks):
+        for b in range(1, blocks):
             moe_sum = moe_sum + weights[:, b : b + 1] * r.returned[b].astype(f32)
         r.out[...] = moe_sum.astype(bf)
 
+    small_first = [slab(units, PIECES, 0), slab(units, PIECES, 1), slab(units, 2, 1)]
     glu_rest()
     shared()
     conv(1, 4)
     pass_on(1, 0, halves[0])
     conv(4, 5)
     swap_wait(1, 0, halves[0])
-    for t in range(2):
-        first(1, halves[0], slab(units, 2, t))
+    for cols in small_first:
+        first(1, halves[0], cols)
     pass_on(1, 1, halves[1])
     pass_on(2)
     pass_on(4, condition=inner)
     relay_edge()
     conv(5, 6)
     swap_wait(1, 1, halves[1])
-    for t in range(2):
-        first(1, halves[1], slab(units, 2, t))
+    for cols in small_first:
+        first(1, halves[1], cols)
     swap_wait(2)
     block_first(2)
     relay(0)
@@ -461,6 +467,7 @@
     for j in range(1, spans):
         send_conv(j)
     shared_down()
+    weigh()
     for b in (7, 5):
         relay(b)
         finish(b)
@@ -579,6 +586,7 @@
         outgoing=pltpu.VMEM((blocks, rows, columns), bf),
         shidden=pltpu.VMEM((TP, rows, shared_gate.shape[1]), bf),
         shared_sum=pltpu.VMEM((rows, columns), f32),
+        weights=pltpu.VMEM((rows, 128), f32),
         load_sem=dma(PIECES + 16),
         e_send=dma(1),
         e_recv=dma(2),

time: 67.7 us -> 67.5 us (level)
  no operation moved by 1% of the time
where the time goes in v4:
time: 67.5 us; the launch traced here: 67.4 us
  Pallas kernels  66.6 us (99%)
  between operations  0.81 us (1%)
    pallas_call x1, Pallas kernels, fused(): pl.pallas_call(functools.partial(layer_kernel, depth, (*operands, *output...  65.7 us

profile of v4, /device:TPU:1, one launch (start us, length us, event | category | flops | bytes accessed | tf_op | source)
XLA Modules:
  0.0 67.4 jit_solution(1213615800652989131)
XLA Ops:
  0.6 65.7 %shard_map.167 = (bf16[512,512]{1,0:T(8,128)(2,1)S(1)}, bf16[128,512]{1,0:T(8,128)(2,1)S(1)}) custom-call(bf16[128,2048]{1,0:T(8,128)(2,1)} %refs_0_.1, bf16[1,2048,1024]{2,1,0:T(8,128)(2,1)} %refs_1_.1, bf16[1,2048,1024]{2,1,0:T(8,128)(2,1)} %refs_2_.1, bf16[1,4096,512]{2,1,0:T(8,128)(2,1)} %refs_3_.1, bf16[2048,128]{1,0:T(8,128)(2,1)} %refs_4_.1, ...), custom_call_target="tpu_custom_call" | custom-call | flops 25769803776 | bytes 40000000 | tf_op jit(solution)/shard_map/pallas_call | solution.py:614
  66.3 0.8 %shard_map.168 = (bf16[512,512]{1,0:T(8,128)(2,1)}, bf16[128,512]{1,0:T(8,128)(2,1)}) custom-call(bf16[512,512]{1,0:T(8,128)(2,1)S(1)} %get-tuple-element.4.conv_done, bf16[128,512]{1,0:T(8,128)(2,1)S(1)} %get-tuple-element.5.done), custom_call_target="tpu_custom_call" | custom-call | tf_op jit(solution)/shard_map/pallas_call | solution.py:625
